TPU v7x, 32 devices: a whole 2x2x4 slice. The times are simulated.
32 devices in a mesh: fs: 8 (over z, y), tp: 4 (over x, core).
Axes of the slice: x: 2, y: 2, z: 4, core: 2. Of those that a mesh axis runs over, the one named last changes fastest.
Arguments:
- tokens: bfloat16 [8192, 2048], P('fs', 'tp'), may hold values from -6 to 6
- norm_gain: float32 [2048], P('fs'), may hold values from 0.1 to 1.9
- up_master: float32 [2048, 8192], P('fs', 'tp'), may hold values from -0.125 to 0.125
- down_master: float32 [2048, 8192], P('fs', 'tp'), may hold values from -0.0625 to 0.0625
Outputs:
- up_weights: bfloat16 [2048, 8192], P(None, 'tp')
- down_weights: bfloat16 [8192, 2048], P('tp')
- mlp_out: bfloat16 [8192, 2048], P('fs', 'tp')
All inputs are finite; a program needn't handle non-finite values.
Results may differ from a plain program's by a relative error of at most 0.014.
Values may be sent and summed in bfloat16 or wider, within the bound.
A program may use at most 128 MiB of HBM per device.

v0:
```python
import functools

import jax
import jax.numpy as jnp
from jax import lax
from jax.experimental import pallas as pl
from jax.experimental.pallas import tpu as pltpu
from jax.sharding import PartitionSpec as P

norm_floor = 1e-06
MESH = pl.DeviceIdType.MESH


def grid_of(n):
    ny = max(d for d in range(1, n + 1) if n % d == 0 and d * d <= n)
    return n // ny, ny


def position_of(f, nz, ny):
    if ny == 1:
        return f
    z, y = lax.div(f, ny), lax.rem(f, ny)
    tail = lax.div(y + (ny - 1), ny)
    k = nz - 1 - z
    odd = lax.rem(k, 2)
    r = (1 - odd) * (y - 1) + odd * (ny - 1 - y)
    return (1 - tail) * z + tail * (nz + k * (ny - 1) + r)


def index_at(p, nz, ny):
    if ny == 1:
        return p
    tail = lax.div(lax.div(p, nz) + (ny - 2), ny - 1)
    q = tail * (p - nz)
    k = lax.div(q, ny - 1)
    r = lax.rem(q, ny - 1)
    odd = lax.rem(k, 2)
    z = (1 - tail) * p + tail * (nz - 1 - k)
    y = tail * ((1 - odd) * (1 + r) + odd * (ny - 1 - r))
    return z * ny + y


def send_list(n):
    hops = n // 2
    split = n % 2 == 0

    def pieces(a, h):
        return [(a, h, 0)] if split and h == hops - 1 else [(a, h, 0), (a, h, 1)]

    ups = [p for h in range(1, hops) for p in pieces("u", h)]
    downs = [p for h in range(1, hops) for p in pieces("d", h)]
    own_u, own_d = pieces("u", 0), pieces("d", 0)
    return own_u + own_d[:1] + ups + own_d[1:] + downs


def gather_kernel(
    n_fs, n_tp, tokens, gain, up_l, dn_l, up_w, dn_w, recv, x, hid, part, stage, up_f, dn_f, gain_v,
    loc_sem, tok_s, tok_r, ring_s, ring_r, pre_s, pre_r, rs_s, rs_r,
):
    nz, ny = grid_of(n_fs)
    me_f, me_t = lax.axis_index("fs"), lax.axis_index("tp")
    pos = position_of(me_f, nz, ny)
    T, Dk = tokens.shape
    R, F = up_l.shape
    D = n_fs * R
    split_cols = (R // 2) % 128 == 0
    W = R // 2 if split_cols else R

    def at(offset):
        return index_at(lax.rem(pos + offset + n_fs, n_fs), nz, ny)

    right, left = at(1), at(-1)

    def tp_peer(k):
        return lax.rem(me_t + k, n_tp)

    barrier = pltpu.get_barrier_semaphore()
    for f in (right, left):
        pl.semaphore_signal(barrier, inc=1, device_id={"fs": f, "tp": me_t}, device_id_type=MESH)
    for k in range(1, n_tp):
        pl.semaphore_signal(barrier, inc=1, device_id={"fs": me_f, "tp": tp_peer(k)}, device_id_type=MESH)

    def up_piece(f, h):
        return up_w.at[pl.ds(pl.multiple_of(f * R + h * (R // 2), R // 2), R // 2), :]

    def dn_piece(f, h):
        if split_cols:
            return dn_w.at[:, pl.ds(pl.multiple_of(f * R + h * (R // 2), R // 2), R // 2)]
        return dn_w.at[pl.ds(h * (F // 2), F // 2), pl.ds(pl.multiple_of(f * R, R), R)]

    def tok_cols(t):
        return x.at[:, pl.ds(pl.multiple_of(t * Dk, Dk), Dk)]

    own = [
        pltpu.make_async_copy(up_l, up_f, loc_sem.at[0]),
        pltpu.make_async_copy(tokens, tok_cols(me_t), loc_sem.at[1]),
        pltpu.make_async_copy(dn_l, dn_f, loc_sem.at[2]),
    ]
    gain_copy = pltpu.make_async_copy(gain, gain_v, loc_sem.at[3])
    for c in [gain_copy] + own:
        c.start()
    own_rows = pl.ds(pl.multiple_of(me_f * R, R), R)
    gain_copy.wait()
    spread = jnp.transpose(jnp.broadcast_to(gain_v[...], (128, R)))
    own[0].wait()
    for c in range(F // 128):
        cols = pl.ds(c * 128, 128)
        up_w[own_rows, cols] = (spread * up_f[:, cols]).astype(jnp.bfloat16)
    own[1].wait()
    pl.semaphore_wait(barrier, n_tp + 1)

    order = send_list(n_fs)
    S = len(order)

    def ring_copy(s, d):
        a, hop, second = order[s]
        half = second if d == 0 else 1 - second
        f = at(-hop if d == 0 else hop)
        ref = up_piece(f, half) if a == "u" else dn_piece(f, half)
        return pltpu.make_async_remote_copy(
            src_ref=ref, dst_ref=ref, send_sem=ring_s.at[d, s], recv_sem=ring_r.at[d, s],
            device_id={"fs": right if d == 0 else left, "tp": me_t}, device_id_type=MESH,
        )

    def arrival(s, d):
        a, hop, second = order[s]
        half = second if d == 0 else 1 - second
        f = at(-(hop + 1) if d == 0 else hop + 1)
        return f, half, (up_piece(f, half) if a == "u" else dn_piece(f, half))

    def wait_arrival(s, d):
        f, half, ref = arrival(s, d)
        pltpu.make_async_remote_copy(
            src_ref=ref, dst_ref=ref, send_sem=ring_s.at[d, s], recv_sem=ring_r.at[d, s],
            device_id={"fs": right if d == 0 else left, "tp": me_t}, device_id_type=MESH,
        ).wait_recv()

    needs = [-1 if hop == 0 else order.index((a, hop - 1, second)) for a, hop, second in order]
    issued = [0]

    def issue(upto):
        while issued[0] < S and needs[issued[0]] <= upto:
            if upto < 0 and issued[0] >= 3:
                break
            for d in range(2):
                ring_copy(issued[0], d).start()
            issued[0] += 1

    for s in range(2):
        for d in range(2):
            ring_copy(s, d).start()

    def token_copy(k):
        return pltpu.make_async_remote_copy(
            src_ref=tok_cols(me_t), dst_ref=tok_cols(me_t), send_sem=tok_s.at[k], recv_sem=tok_r.at[k],
            device_id={"fs": me_f, "tp": tp_peer(k)}, device_id_type=MESH,
        )

    for k in range(1, n_tp):
        token_copy(k).start()
    own[2].wait()
    block = min(F, 256)

    @pl.loop(0, F // block)
    def _(i):
        r = pl.ds(pl.multiple_of(i * block, block), block)
        dn_w[r, own_rows] = jnp.transpose(dn_f[:, r]).astype(jnp.bfloat16)

    issued[0] = 2
    issue(-1)

    def normalise():
        for k in range(1, n_tp):
            src = lax.rem(me_t - k + n_tp, n_tp)
            pltpu.make_async_remote_copy(
                src_ref=tok_cols(src), dst_ref=tok_cols(src), send_sem=tok_s.at[k], recv_sem=tok_r.at[k],
                device_id={"fs": me_f, "tp": tp_peer(k)}, device_id_type=MESH,
            ).wait_recv()
            token_copy(k).wait_send()
        rows = 64

        @pl.loop(0, T // rows)
        def _(i):
            r = pl.ds(pl.multiple_of(i * rows, rows), rows)
            v = x[r, :].astype(jnp.float32)
            x[r, :] = (v * lax.rsqrt(jnp.mean(v * v, axis=-1, keepdims=True) + norm_floor)).astype(jnp.bfloat16)

    def make_hidden():
        width = 256

        @pl.loop(0, F // width)
        def _(i):
            c = pl.ds(pl.multiple_of(i * width, width), width)
            pre = jnp.dot(x[...], up_w[:, c], preferred_element_type=jnp.float32)
            hid[:, c] = jnp.square(jnp.maximum(pre, 0.0)).astype(jnp.bfloat16)

    per_owner = Dk // W
    nx = n_tp // 2
    half_rows = T // 2
    me_x, me_c = lax.div(me_t, 2), lax.rem(me_t, 2)
    sibling = me_t + 1 - 2 * me_c
    my_half = pl.ds(pl.multiple_of(me_c * half_rows, half_rows), half_rows)
    its_half = pl.ds(pl.multiple_of((1 - me_c) * half_rows, half_rows), half_rows)

    def device(t):
        return dict(device_id={"fs": me_f, "tp": t}, device_id_type=MESH)

    def cols_of(q):
        return pl.ds(pl.multiple_of(lax.rem(q, per_owner) * W, W), W)

    def whole_copy(q):
        return pltpu.make_async_remote_copy(
            src_ref=part.at[q], dst_ref=recv.at[nx, :, cols_of(q)],
            send_sem=rs_s.at[q], recv_sem=rs_r.at[nx, lax.rem(q, per_owner), 0], **device(sibling),
        )

    def pair_copy(q):
        return pltpu.make_async_remote_copy(
            src_ref=part.at[q, its_half], dst_ref=stage.at[q],
            send_sem=pre_s.at[q], recv_sem=pre_r.at[q], **device(sibling),
        )

    def half_copy(q):
        return pltpu.make_async_remote_copy(
            src_ref=part.at[q, my_half], dst_ref=recv.at[me_x, my_half, cols_of(q)],
            send_sem=rs_s.at[q], recv_sem=rs_r.at[me_x, lax.rem(q, per_owner), me_c],
            **device(lax.div(q, per_owner)),
        )

    def pass_on(q):
        @pl.when(lax.div(q, 2 * per_owner) != me_x)
        def _():
            pair_copy(q).wait_recv()
            both = part[q, my_half, :].astype(jnp.float32) + stage[q].astype(jnp.float32)
            part[q, my_half, :] = both.astype(jnp.bfloat16)
            half_copy(q).start()

    def do_parts(first, count):
        c = pl.ds(pl.multiple_of(first * W, W), count * W)

        @pl.loop(0, 2)
        def _(i):
            r = pl.ds(pl.multiple_of(lax.rem(i + 1 + me_c, 2) * half_rows, half_rows), half_rows)
            out = jnp.dot(hid[r, :], dn_w[:, c], preferred_element_type=jnp.float32).astype(jnp.bfloat16)
            for k in range(count):
                part[first + k, r, :] = out[:, k * W : (k + 1) * W]
            for k in range(count):
                owner = lax.div(first + k, per_owner)

                @pl.when((i == 0) & (lax.div(owner, 2) != me_x))
                def _():
                    pair_copy(first + k).start()

                @pl.when((i == 1) & (owner == sibling))
                def _():
                    whole_copy(first + k).start()

    per_chunk = R // W
    ready = [(me_f * per_chunk, per_chunk)]
    last_up = max(s for s in range(S) if order[s][0] == "u")
    norm_at = max(0, last_up - 2)
    for s in range(S):
        for d in range(2):
            wait_arrival(s, d)
        issue(s)
        a, hop, _ = order[s]
        if a == "d" and split_cols:
            if n_fs % 2 == 0 and hop == n_fs // 2 - 1:
                ready.append((at(hop + 1) * 2, 2))
            else:
                for d in range(2):
                    f, half, _ = arrival(s, d)
                    ready.append((f * 2 + half, 1))
        if s == norm_at:
            normalise()
        if s == last_up:
            make_hidden()
        if s >= last_up:
            for first, count in ready:
                do_parts(first, count)
            for first, count in ready:
                for k in range(count):
                    pass_on(first + k)
            ready = []
    if not split_cols:
        @pl.loop(0, n_fs)
        def _(q):
            @pl.when(q != me_f)
            def _():
                do_parts(q, 1)
                pass_on(q)

    @pl.loop(0, per_owner)
    def _(local):
        cols = pl.ds(pl.multiple_of(local * W, W), W)
        recv[me_x, :, cols] = part[me_t * per_owner + local]

    for d in range(2):
        for s in range(S):
            ring_copy(s, d).wait_send()

    @pl.loop(0, D // W)
    def _(q):
        owner = lax.div(q, per_owner)

        @pl.when(owner == sibling)
        def _():
            whole_copy(q).wait_send()

        @pl.when(lax.div(owner, 2) != me_x)
        def _():
            pair_copy(q).wait_send()
            half_copy(q).wait_send()

    for local in range(per_owner):
        q = me_t * per_owner + local
        whole_copy(q).wait_recv()
        for k in range(1, nx):
            src = lax.rem(me_x + k, nx)
            for c in range(2):
                ref = recv.at[src, pl.ds(c * half_rows, half_rows), pl.ds(local * W, W)]
                pltpu.make_async_remote_copy(
                    src_ref=ref, dst_ref=ref, send_sem=rs_s.at[0], recv_sem=rs_r.at[src, local, c], **device(sibling),
                ).wait_recv()


def finish_kernel(up_v, dn_v, recv, up_o, dn_o, mlp_o, total, sem):
    copies = [pltpu.make_async_copy(up_v, up_o, sem.at[0]), pltpu.make_async_copy(dn_v, dn_o, sem.at[1])]
    for c in copies:
        c.start()
    n, T, _ = recv.shape
    rows = 128

    @pl.loop(0, T // rows)
    def _(i):
        r = pl.ds(pl.multiple_of(i * rows, rows), rows)
        acc = recv[0, r, :].astype(jnp.float32)
        for k in range(1, n):
            acc += recv[k, r, :].astype(jnp.float32)
        total[r, :] = acc.astype(jnp.bfloat16)

    last = pltpu.make_async_copy(total, mlp_o, sem.at[2])
    last.start()
    for c in copies:
        c.wait()
    last.wait()


def solution(mesh):
    n_fs, n_tp = mesh.shape["fs"], mesh.shape["tp"]
    bf16 = jnp.bfloat16

    def on_device(tokens, norm_gain, up_master, down_master):
        T, Dk = tokens.shape
        R, F = up_master.shape
        D = n_fs * R
        W = R // 2 if (R // 2) % 128 == 0 else R
        S = len(send_list(n_fs))
        any_spec = pl.BlockSpec(memory_space=pl.ANY)
        vmem_spec = pl.BlockSpec(memory_space=pltpu.VMEM)
        up_v, dn_v, recv = pl.pallas_call(
            functools.partial(gather_kernel, n_fs, n_tp),
            out_shape=(pltpu.VMEM((D, F), bf16), pltpu.VMEM((F, D), bf16), pltpu.VMEM((n_tp // 2 + 1, T, Dk), bf16)),
            in_specs=[pl.BlockSpec(memory_space=pltpu.HBM)] * 4,
            out_specs=(vmem_spec,) * 3,
            scratch_shapes=[
                pltpu.VMEM((T, D), bf16),
                pltpu.VMEM((T, F), bf16),
                pltpu.VMEM((D // W, T, W), bf16),
                pltpu.VMEM((D // W, T // 2, W), bf16),
                pltpu.VMEM((R, F), jnp.float32),
                pltpu.VMEM((R, F), jnp.float32),
                pltpu.VMEM((1, R), jnp.float32),
                pltpu.SemaphoreType.DMA((4,)),
                pltpu.SemaphoreType.DMA((n_tp,)),
                pltpu.SemaphoreType.DMA((n_tp,)),
                pltpu.SemaphoreType.DMA((2, S)),
                pltpu.SemaphoreType.DMA((2, S)),
                pltpu.SemaphoreType.DMA((D // W,)),
                pltpu.SemaphoreType.DMA((D // W,)),
                pltpu.SemaphoreType.DMA((D // W,)),
                pltpu.SemaphoreType.DMA((n_tp // 2 + 1, Dk // W, 2)),
            ],
            compiler_params=pltpu.CompilerParams(
                collective_id=0, has_side_effects=True, vmem_limit_bytes=44 * 2**20
            ),
        )(tokens, norm_gain[None, :], up_master, down_master)
        return pl.pallas_call(
            finish_kernel,
            out_shape=(
                jax.ShapeDtypeStruct((D, F), bf16),
                jax.ShapeDtypeStruct((F, D), bf16),
                jax.ShapeDtypeStruct((T, Dk), bf16),
            ),
            in_specs=[vmem_spec] * 3,
            out_specs=(any_spec,) * 3,
            scratch_shapes=[pltpu.VMEM((T, Dk), bf16), pltpu.SemaphoreType.DMA((3,))],
            compiler_params=pltpu.CompilerParams(vmem_limit_bytes=8 * 2**20),
        )(up_v, dn_v, recv)

    in_specs = (P("fs", "tp"), P("fs"), P("fs", "tp"), P("fs", "tp"))
    out_specs = (P(None, "tp"), P("tp", None), P("fs", "tp"))
    return jax.shard_map(on_device, mesh=mesh, in_specs=in_specs, out_specs=out_specs, check_vma=False)
```

profile of v0, /device:TPU:1, one launch (start us, length us, event | category | flops | bytes accessed | tf_op | source)
XLA Modules:
  0.0 178.8 jit_solution(17146898356240857918)
XLA Ops:
  0.6 171.9 %shard_map.67 = (bf16[2048,2048]{1,0:T(8,128)(2,1)S(1)}, bf16[2048,2048]{1,0:T(8,128)(2,1)S(1)}, bf16[3,1024,512]{2,1,0:T(8,128)(2,1)S(1)}) custom-call(bf16[1024,512]{1,0:T(8,128)(2,1)} %tokens.1, f32[1,256]{1,0:T(1,128)} %bitcast.1, f32[256,2048]{1,0:T(8,128)} %up_l.1, f32[256,2048]{1,0:T(8,128)} %dn_l.1), custom_call_target="tpu_custom_call" | custom-call | tf_op jit(solution)/shard_map/pallas_call | solution.py:361
  172.5 6.3 %shard_map.68 = (bf16[2048,2048]{1,0:T(8,128)(2,1)}, bf16[2048,2048]{1,0:T(8,128)(2,1)}, bf16[1024,512]{1,0:T(8,128)(2,1)}) custom-call(bf16[2048,2048]{1,0:T(8,128)(2,1)S(1)} %get-tuple-element.6.up_v, bf16[2048,2048]{1,0:T(8,128)(2,1)S(1)} %get-tuple-element.7.dn_v, bf16[3,1024,512]{2,1,0:T(8,128)(2,1)S(1)} %get-tuple-element.8.recv), custom_call_target="tpu_custom_call" | custom-call | tf_op jit(solution)/shard_map/pallas_call | solution.py:388
where the time goes:
time: 180 us; the launch traced here: 179 us
  Pallas kernels  178 us (99%)
    pallas_call x1, Pallas kernels, on_device(): pl.pallas_call(functools.partial(gather_kernel, n_fs, n_tp), out_shape=(p...  172 us
    pallas_call x1, Pallas kernels, on_device(): pl.pallas_call(finish_kernel, out_shape=(jax.ShapeDtypeStruct((D, F), bf1...  6.28 us

commit v1 on v0

--- a/solution.py
+++ b/solution.py
@@ -324,6 +324,414 @@
                 ).wait_recv()
 
 
+slot_kinds = "UUDUUDUUUDDDDD"
+slot_pieces = (
+    0xECA86420, 0xFDB97531,
+    0xECA96420, 0xCA86420E,
+    0xDB97531F, 0xCAB87501,
+    0xA86420EC, 0xB97531FD,
+    0x86420ECA, 0xAB87423E,
+    0xB896501C, 0x897423EA,
+    0x926501F0, 0xFD023EC0,
+)
+slot_live = (0xFF, 0xFF, 0xFF, 0xFF, 0xFF, 0xFF, 0xFF, 0xFF, 0xFF, 0xFF, 0xFF, 0xFF, 0xFE, 0xDE)
+slot_ahead = (1, 2, 2, 2, 2, 2, 2, 2, 2, 2, 1, 1, 1, 2)
+relays = ((1, 13), (4, 15), (7, 11))
+relay_place = 6
+ring_places = 8
+last_chunks = 4
+tiles_per_step = 3
+
+
+def look(word, place, width):
+    word = word - 2**32 if word >= 2**31 else word
+    return lax.bitwise_and(lax.shift_right_logical(jnp.int32(word), place * width), jnp.int32(2**width - 1))
+
+
+def routed_kernel(
+    n_fs, n_tp, tokens, gain, up_l, dn_l, up_w, dn_w, recv, x, hid, part, stage, up_f, dn_f, gain_v, acc,
+    loc_sem, tok_s, tok_r, ring_s, ring_r, y_s, y_r, pre_s, pre_r, rs_s, rs_r,
+):
+    nz, ny = grid_of(n_fs)
+    me_f, me_t = lax.axis_index("fs"), lax.axis_index("tp")
+    T, Dk = tokens.shape
+    R, F = up_l.shape
+    D = n_fs * R
+    W = R // 2
+    nx = n_tp // 2
+    me_x, me_c = lax.div(me_t, 2), lax.rem(me_t, 2)
+    sibling = me_t + 1 - 2 * me_c
+    half_rows = T // 2
+    per_owner = Dk // W
+    S = len(slot_kinds)
+    last = S - 1
+
+    mz, my = lax.div(me_f, ny), lax.rem(me_f, ny)
+    lane = mz + me_x * (nz - 1 - 2 * mz)
+    pos = lane + my * (n_fs - 1 - 2 * lane)
+
+    def at(p):
+        side = lax.div(p, nz)
+        along = p + side * (n_fs - 1 - 2 * p)
+        return (along + me_x * (nz - 1 - 2 * along)) * ny + side
+
+    right, left, across = at(lax.rem(pos + 1, n_fs)), at(lax.rem(pos + n_fs - 1, n_fs)), at(n_fs - 1 - pos)
+    seat = (pos, n_fs - 1 - pos)
+    behind = tuple(lax.rem(p + n_fs - 1, n_fs) for p in seat)
+    is_relay = (pos == relay_place) | (pos == n_fs - 1 - relay_place)
+
+    def tp_peer(k):
+        return lax.rem(me_t + k, n_tp)
+
+    barrier = pltpu.get_barrier_semaphore()
+    for f in (right, left, across):
+        pl.semaphore_signal(barrier, inc=1, device_id={"fs": f, "tp": me_t}, device_id_type=MESH)
+    for k in range(1, n_tp):
+        pl.semaphore_signal(barrier, inc=1, device_id={"fs": me_f, "tp": tp_peer(k)}, device_id_type=MESH)
+
+    def tok_cols(t):
+        return x.at[:, pl.ds(pl.multiple_of(t * Dk, Dk), Dk)]
+
+    gain_copy = pltpu.make_async_copy(gain, gain_v, loc_sem.at[0])
+    up_copies = [
+        pltpu.make_async_copy(up_l.at[pl.ds(h * W, W), :], up_f.at[pl.ds(h * W, W), :], loc_sem.at[1 + h]) for h in range(2)
+    ]
+    tok_copy = pltpu.make_async_copy(tokens, tok_cols(me_t), loc_sem.at[3])
+    dn_copy = pltpu.make_async_copy(dn_l, dn_f, loc_sem.at[4])
+    for c in [gain_copy] + up_copies + [dn_copy, tok_copy]:
+        c.start()
+
+    def mirrored(code, m):
+        src, half = lax.div(code, 2), lax.rem(code, 2)
+        return at(src + m * (n_fs - 1 - 2 * src)), half + m * (1 - 2 * half)
+
+    def piece(s, place, d):
+        return mirrored(look(slot_pieces[s], place, 4), d)
+
+    def live(s, place):
+        return None if slot_live[s] == 2**n_fs - 1 else look(slot_live[s], place, 1) == 1
+
+    def when(pred, body):
+        if pred is None:
+            body()
+        else:
+            pl.when(pred)(body)
+
+    def chunks(s):
+        return last_chunks if s == last else 2
+
+    def index(s, c):
+        return 2 * s + c
+
+    def ref_of(kind, f, half, c, n):
+        if kind == "U":
+            rows = W // n
+            return up_w.at[pl.ds(pl.multiple_of(f * R + half * W + c * rows, rows), rows), :]
+        return dn_w.at[pl.ds(c * (F // n), F // n), pl.ds(pl.multiple_of(f * R + half * W, W), W)]
+
+    def ring_copy(s, c, d, place):
+        f, half = piece(s, place, d)
+        ref = ref_of(slot_kinds[s], f, half, c, chunks(s))
+        return pltpu.make_async_remote_copy(
+            src_ref=ref, dst_ref=ref, send_sem=ring_s.at[d, index(s, c)], recv_sem=ring_r.at[d, index(s, c)],
+            device_id={"fs": right if d == 0 else left, "tp": me_t}, device_id_type=MESH,
+        )
+
+    def send(s, c):
+        for d in range(2):
+            when(live(s, seat[d]), lambda: ring_copy(s, c, d, seat[d]).start())
+
+    def arrive(s, c):
+        for d in range(2):
+            when(live(s, behind[d]), lambda: ring_copy(s, c, d, behind[d]).wait_recv())
+
+    def relay_copy(j, m):
+        f, half = mirrored(jnp.int32(relays[j][1]), m)
+        ref = ref_of("D", f, half, 0, 1)
+        return pltpu.make_async_remote_copy(
+            src_ref=ref, dst_ref=ref, send_sem=y_s.at[j], recv_sem=y_r.at[j],
+            device_id={"fs": across, "tp": me_t}, device_id_type=MESH,
+        )
+
+    relay_out = jnp.where(pos == relay_place, 0, 1)
+
+    own_row = pl.multiple_of(me_f * R, R)
+    gain_copy.wait()
+    spread = jnp.transpose(jnp.broadcast_to(gain_v[...], (128, R)))
+    for h in range(2):
+        up_copies[h].wait()
+        for c in range(F // 128):
+            cols = pl.ds(c * 128, 128)
+            up_w[pl.ds(own_row + h * W, W), cols] = (
+                spread[h * W : (h + 1) * W] * up_f[pl.ds(h * W, W), cols]
+            ).astype(jnp.bfloat16)
+    pl.semaphore_wait(barrier, n_tp + 2)
+    for t in range(2):
+        if t < slot_ahead[t]:
+            for e in range(2):
+                send(t, e)
+
+    def token_copy(k):
+        return pltpu.make_async_remote_copy(
+            src_ref=tok_cols(me_t), dst_ref=tok_cols(me_t), send_sem=tok_s.at[k], recv_sem=tok_r.at[k],
+            device_id={"fs": me_f, "tp": tp_peer(k)}, device_id_type=MESH,
+        )
+
+    tok_copy.wait()
+    for k in range(1, n_tp):
+        token_copy(k).start()
+    dn_copy.wait()
+    block = min(F, 256)
+
+    @pl.loop(0, F // block)
+    def _(i):
+        r = pl.ds(pl.multiple_of(i * block, block), block)
+        dn_w[r, pl.ds(own_row, R)] = jnp.transpose(dn_f[:, r]).astype(jnp.bfloat16)
+
+    def normalise():
+        for k in range(1, n_tp):
+            src = lax.rem(me_t - k + n_tp, n_tp)
+            pltpu.make_async_remote_copy(
+                src_ref=tok_cols(src), dst_ref=tok_cols(src), send_sem=tok_s.at[k], recv_sem=tok_r.at[k],
+                device_id={"fs": me_f, "tp": tp_peer(k)}, device_id_type=MESH,
+            ).wait_recv()
+            token_copy(k).wait_send()
+        rows = 64
+
+        @pl.loop(0, T // rows)
+        def _(i):
+            r = pl.ds(pl.multiple_of(i * rows, rows), rows)
+            v = x[r, :].astype(jnp.float32)
+            x[r, :] = (v * lax.rsqrt(jnp.mean(v * v, axis=-1, keepdims=True) + norm_floor)).astype(jnp.bfloat16)
+
+    width = 256
+
+    def make_hidden(first, count):
+        @pl.loop(first, first + count)
+        def _(i):
+            c = pl.ds(pl.multiple_of(i * width, width), width)
+            pre = jnp.dot(x[...], up_w[:, c], preferred_element_type=jnp.float32)
+            hid[:, c] = jnp.square(jnp.maximum(pre, 0.0)).astype(jnp.bfloat16)
+
+    my_half = pl.ds(pl.multiple_of(me_c * half_rows, half_rows), half_rows)
+    its_half = pl.ds(pl.multiple_of((1 - me_c) * half_rows, half_rows), half_rows)
+
+    def device(t):
+        return dict(device_id={"fs": me_f, "tp": t}, device_id_type=MESH)
+
+    def cols_of(q):
+        return pl.ds(pl.multiple_of(lax.rem(q, per_owner) * W, W), W)
+
+    def tile(q):
+        return pl.ds(pl.multiple_of(q * W, W), W)
+
+    def whole_copy(q):
+        return pltpu.make_async_remote_copy(
+            src_ref=part.at[q], dst_ref=recv.at[nx, :, cols_of(q)],
+            send_sem=rs_s.at[q], recv_sem=rs_r.at[nx, lax.rem(q, per_owner), 0], **device(sibling),
+        )
+
+    def pair_copy(q):
+        return pltpu.make_async_remote_copy(
+            src_ref=part.at[q, its_half], dst_ref=stage.at[q],
+            send_sem=pre_s.at[q], recv_sem=pre_r.at[q], **device(sibling),
+        )
+
+    def half_copy(q):
+        return pltpu.make_async_remote_copy(
+            src_ref=part.at[q, my_half], dst_ref=recv.at[me_x, my_half, cols_of(q)],
+            send_sem=rs_s.at[q], recv_sem=rs_r.at[me_x, lax.rem(q, per_owner), me_c],
+            **device(lax.div(q, per_owner)),
+        )
+
+    def pass_on(q):
+        @pl.when(lax.div(q, 2 * per_owner) != me_x)
+        def _():
+            pair_copy(q).wait_recv()
+            both = part[q, my_half, :].astype(jnp.float32) + stage[q].astype(jnp.float32)
+            part[q, my_half, :] = both.astype(jnp.bfloat16)
+            half_copy(q).start()
+
+    def do_part(q):
+        owner = lax.div(q, per_owner)
+
+        @pl.loop(0, 2)
+        def _(i):
+            r = pl.ds(pl.multiple_of(lax.rem(i + 1 + me_c, 2) * half_rows, half_rows), half_rows)
+            part[q, r, :] = jnp.dot(hid[r, :], dn_w[:, tile(q)], preferred_element_type=jnp.float32).astype(jnp.bfloat16)
+
+            @pl.when((i == 0) & (lax.div(owner, nx) != me_x))
+            def _():
+                pair_copy(q).start()
+
+            @pl.when((i == 1) & (owner == sibling))
+            def _():
+                whole_copy(q).start()
+
+    def entry_of(e):
+        kind = e[0]
+        if kind == "none":
+            return jnp.int32(0), jnp.int32(0)
+        if kind == "own":
+            return me_f * 2 + e[1], jnp.int32(1)
+        if kind == "relay":
+            f, half = mirrored(jnp.int32(relays[e[1]][1]), 1 - relay_out)
+            return f * 2 + half, jnp.where(is_relay, 1, 0)
+        s, d = e[1], e[2]
+        f, half = piece(s, behind[d], d)
+        ok = jnp.int32(1) if slot_live[s] == 2**n_fs - 1 else look(slot_live[s], behind[d], 1)
+        return f * 2 + half, ok
+
+    def pick(i, values):
+        out = values[0]
+        for k in range(1, len(values)):
+            out = jnp.where(i == k, values[k], out)
+        return out
+
+    def run_tiles(before, entries):
+        cur = [entry_of(e) for e in entries]
+        prev = [entry_of(before)] + cur[:-1]
+
+        @pl.loop(0, len(entries))
+        def _(i):
+            q = pick(i, [v[0] for v in cur])
+
+            @pl.when(pick(i, [v[1] for v in cur]) == 1)
+            def _():
+                do_part(q)
+
+            p = pick(i, [v[0] for v in prev])
+
+            @pl.when(pick(i, [v[1] for v in prev]) == 1)
+            def _():
+                pass_on(p)
+
+    def tail_tiles(c):
+        tiles = []
+        for d in range(2):
+            f, half = piece(last, behind[d], d)
+            tiles.append(f * 2 + half)
+        rows = half_rows
+        k = pl.ds(c * (F // last_chunks), F // last_chunks)
+
+        def body():
+            both = jnp.concatenate([dn_w[k, tile(q)] for q in tiles], axis=1)
+
+            @pl.loop(0, T // rows)
+            def _(i):
+                r = pl.ds(pl.multiple_of(i * rows, rows), rows)
+                out = jnp.dot(hid[r, k], both, preferred_element_type=jnp.float32)
+                if c > 0:
+                    out += acc[r, :]
+                if c < last_chunks - 1:
+                    acc[r, :] = out
+                else:
+                    for j, q in enumerate(tiles):
+                        part[q, r, :] = out[:, j * W : (j + 1) * W].astype(jnp.bfloat16)
+
+            if c == last_chunks - 1:
+                for q in tiles:
+                    @pl.when(lax.div(q, per_owner) == sibling)
+                    def _():
+                        whole_copy(q).start()
+
+        when(live(last, behind[0]), body)
+
+    def send_after(t, e):
+        if t == last:
+            return (t - 1, 0)
+        return (t - slot_ahead[t], e)
+
+    queue = [("own", h) for h in range(2)]
+    hidden_from = 2 * max(s for s in range(S) if slot_kinds[s] == "U") + 1
+    blocks = F // width
+    per_step = (blocks + 1) // 2
+    prior = ("none",)
+    normal_at = max(0, hidden_from - 6)
+
+    for s in range(S):
+        for c in range(chunks(s)):
+            k = index(s, c)
+            arrive(s, c)
+            for j, (t, _) in enumerate(relays):
+                if t + 1 == s and c == 0:
+                    @pl.when(is_relay)
+                    def _():
+                        relay_copy(j, 1 - relay_out).wait_recv()
+                    queue.append(("relay", j))
+            for t in range(s + 1, S):
+                for e in range(chunks(t)):
+                    if send_after(t, e) == (s, c):
+                        send(t, e)
+            if c == 1 and s < last:
+                for j, (t, _) in enumerate(relays):
+                    if t == s + 1:
+                        @pl.when(is_relay)
+                        def _():
+                            relay_copy(j, relay_out).start()
+                if slot_kinds[s] == "D":
+                    queue += [("ring", s, d) for d in range(2)]
+            if k == normal_at:
+                normalise()
+            if k in (hidden_from, hidden_from + 1):
+                make_hidden((k - hidden_from) * per_step, min(per_step, blocks - (k - hidden_from) * per_step))
+            if k > hidden_from + 1 and (s, c) < (last - 1, 1) and queue:
+                take = queue[:tiles_per_step]
+                queue = queue[tiles_per_step:]
+                run_tiles(prior, take)
+                prior = take[-1]
+            if (s, c) == (last - 1, 1):
+                if queue:
+                    run_tiles(prior, queue)
+                    prior = queue[-1]
+                    queue = []
+                q, ok = entry_of(prior)
+
+                @pl.when(ok == 1)
+                def _():
+                    pass_on(q)
+            if s == last:
+                tail_tiles(c)
+
+    @pl.loop(0, per_owner)
+    def _(local):
+        cols = pl.ds(pl.multiple_of(local * W, W), W)
+        recv[me_x, :, cols] = part[me_t * per_owner + local]
+
+    for s in range(S):
+        for c in range(chunks(s)):
+            for d in range(2):
+                when(live(s, seat[d]), lambda: ring_copy(s, c, d, seat[d]).wait_send())
+    for j in range(len(relays)):
+        @pl.when(is_relay)
+        def _():
+            relay_copy(j, relay_out).wait_send()
+
+    @pl.loop(0, D // W)
+    def _(q):
+        owner = lax.div(q, per_owner)
+
+        @pl.when(owner == sibling)
+        def _():
+            whole_copy(q).wait_send()
+
+        @pl.when(lax.div(owner, nx) != me_x)
+        def _():
+            pair_copy(q).wait_send()
+            half_copy(q).wait_send()
+
+    for local in range(per_owner):
+        q = me_t * per_owner + local
+        whole_copy(q).wait_recv()
+        for k in range(1, nx):
+            src = lax.rem(me_x + k, nx)
+            for c in range(2):
+                ref = recv.at[src, pl.ds(c * half_rows, half_rows), pl.ds(local * W, W)]
+                pltpu.make_async_remote_copy(
+                    src_ref=ref, dst_ref=ref, send_sem=rs_s.at[0], recv_sem=rs_r.at[src, local, c], **device(sibling),
+                ).wait_recv()
+
+
 def finish_kernel(up_v, dn_v, recv, up_o, dn_o, mlp_o, total, sem):
     copies = [pltpu.make_async_copy(up_v, up_o, sem.at[0]), pltpu.make_async_copy(dn_v, dn_o, sem.at[1])]
     for c in copies:
@@ -358,8 +766,13 @@
         S = len(send_list(n_fs))
         any_spec = pl.BlockSpec(memory_space=pl.ANY)
         vmem_spec = pl.BlockSpec(memory_space=pltpu.VMEM)
+        routed = (n_fs, grid_of(n_fs)[1], n_tp * grid_of(n_fs)[1], 2 * W) == (ring_places, 2, n_fs, R)
+        waves = 2 * len(slot_kinds) + last_chunks - 2 if routed else S
+        own_sems = 5 if routed else 4
+        extra = [pltpu.VMEM((T, 2 * W), jnp.float32)] if routed else []
+        relay_sems = [pltpu.SemaphoreType.DMA((len(relays),))] * 2 if routed else []
         up_v, dn_v, recv = pl.pallas_call(
-            functools.partial(gather_kernel, n_fs, n_tp),
+            functools.partial(routed_kernel if routed else gather_kernel, n_fs, n_tp),
             out_shape=(pltpu.VMEM((D, F), bf16), pltpu.VMEM((F, D), bf16), pltpu.VMEM((n_tp // 2 + 1, T, Dk), bf16)),
             in_specs=[pl.BlockSpec(memory_space=pltpu.HBM)] * 4,
             out_specs=(vmem_spec,) * 3,
@@ -371,11 +784,13 @@
                 pltpu.VMEM((R, F), jnp.float32),
                 pltpu.VMEM((R, F), jnp.float32),
                 pltpu.VMEM((1, R), jnp.float32),
-                pltpu.SemaphoreType.DMA((4,)),
+                *extra,
+                pltpu.SemaphoreType.DMA((own_sems,)),
                 pltpu.SemaphoreType.DMA((n_tp,)),
                 pltpu.SemaphoreType.DMA((n_tp,)),
-                pltpu.SemaphoreType.DMA((2, S)),
-                pltpu.SemaphoreType.DMA((2, S)),
+                pltpu.SemaphoreType.DMA((2, waves)),
+                pltpu.SemaphoreType.DMA((2, waves)),
+                *relay_sems,
                 pltpu.SemaphoreType.DMA((D // W,)),
                 pltpu.SemaphoreType.DMA((D // W,)),
                 pltpu.SemaphoreType.DMA((D // W,)),

time: 180 us -> 174 us (0.967)
  Pallas kernels: 178 us -> 173 us
    pallas_call x1, Pallas kernels: 172 us -> 167 us  [on_device(): pl.pallas_call(functools.partial(routed_kernel if routed else gather_kern...]
where the time goes in v1:
time: 174 us; the launch traced here: 173 us
  Pallas kernels  173 us (99%)
    pallas_call x1, Pallas kernels, on_device(): pl.pallas_call(functools.partial(routed_kernel if routed else gather_kern...  167 us
    pallas_call x1, Pallas kernels, on_device(): pl.pallas_call(finish_kernel, out_shape=(jax.ShapeDtypeStruct((D, F), bf1...  6.28 us

profile of v1, /device:TPU:1, one launch (start us, length us, event | category | flops | bytes accessed | tf_op | source)
XLA Modules:
  0.0 173.5 jit_solution(15745647970074818397)
XLA Ops:
  0.6 166.5 %shard_map.67 = (bf16[2048,2048]{1,0:T(8,128)(2,1)S(1)}, bf16[2048,2048]{1,0:T(8,128)(2,1)S(1)}, bf16[3,1024,512]{2,1,0:T(8,128)(2,1)S(1)}) custom-call(bf16[1024,512]{1,0:T(8,128)(2,1)} %tokens.1, f32[1,256]{1,0:T(1,128)} %bitcast.1, f32[256,2048]{1,0:T(8,128)} %up_l.1, f32[256,2048]{1,0:T(8,128)} %dn_l.1), custom_call_target="tpu_custom_call" | custom-call | tf_op jit(solution)/shard_map/pallas_call | solution.py:774
  167.2 6.3 %shard_map.68 = (bf16[2048,2048]{1,0:T(8,128)(2,1)}, bf16[2048,2048]{1,0:T(8,128)(2,1)}, bf16[1024,512]{1,0:T(8,128)(2,1)}) custom-call(bf16[2048,2048]{1,0:T(8,128)(2,1)S(1)} %get-tuple-element.6.up_v, bf16[2048,2048]{1,0:T(8,128)(2,1)S(1)} %get-tuple-element.7.dn_v, bf16[3,1024,512]{2,1,0:T(8,128)(2,1)S(1)} %get-tuple-element.8.recv), custom_call_target="tpu_custom_call" | custom-call | tf_op jit(solution)/shard_map/pallas_call | solution.py:803

commit v2 on v1

--- a/solution.py
+++ b/solution.py
@@ -324,6 +324,28 @@
                 ).wait_recv()
 
 
+def finish_kernel(up_v, dn_v, recv, up_o, dn_o, mlp_o, total, sem):
+    copies = [pltpu.make_async_copy(up_v, up_o, sem.at[0]), pltpu.make_async_copy(dn_v, dn_o, sem.at[1])]
+    for c in copies:
+        c.start()
+    n, T, _ = recv.shape
+    rows = 128
+
+    @pl.loop(0, T // rows)
+    def _(i):
+        r = pl.ds(pl.multiple_of(i * rows, rows), rows)
+        acc = recv[0, r, :].astype(jnp.float32)
+        for k in range(1, n):
+            acc += recv[k, r, :].astype(jnp.float32)
+        total[r, :] = acc.astype(jnp.bfloat16)
+
+    last = pltpu.make_async_copy(total, mlp_o, sem.at[2])
+    last.start()
+    for c in copies:
+        c.wait()
+    last.wait()
+
+
 slot_kinds = "UUDUUDUUUDDDDD"
 slot_pieces = (
     0xECA86420, 0xFDB97531,
@@ -340,7 +362,8 @@
 relay_place = 6
 ring_places = 8
 last_chunks = 4
-tiles_per_step = 3
+second_leads = 0x84
+pairs_per_step = 2
 
 
 def look(word, place, width):
@@ -348,36 +371,61 @@
     return lax.bitwise_and(lax.shift_right_logical(jnp.int32(word), place * width), jnp.int32(2**width - 1))
 
 
+class Places:
+    def __init__(self, n_fs, n_tp):
+        nz, ny = grid_of(n_fs)
+        self.n, self.nz, self.ny = n_fs, nz, ny
+        self.me_f, self.me_t = lax.axis_index("fs"), lax.axis_index("tp")
+        self.me_x, self.me_c = lax.div(self.me_t, 2), lax.rem(self.me_t, 2)
+        z, y = lax.div(self.me_f, ny), lax.rem(self.me_f, ny)
+        along = z + self.me_x * (nz - 1 - 2 * z)
+        self.pos = along + y * (n_fs - 1 - 2 * along)
+        self.seat = (self.pos, n_fs - 1 - self.pos)
+        self.behind = tuple(lax.rem(p + n_fs - 1, n_fs) for p in self.seat)
+
+    def at(self, p):
+        side = lax.div(p, self.nz)
+        along = p + side * (self.n - 1 - 2 * p)
+        return (along + self.me_x * (self.nz - 1 - 2 * along)) * self.ny + side
+
+    def mirrored(self, code, m):
+        src, half = lax.div(code, 2), lax.rem(code, 2)
+        return self.at(src + m * (self.n - 1 - 2 * src)), half + m * (1 - 2 * half)
+
+    def piece(self, s, place, d):
+        return self.mirrored(look(slot_pieces[s], place, 4), d)
+
+    def live(self, s, place):
+        return None if slot_live[s] == 2**self.n - 1 else look(slot_live[s], place, 1) == 1
+
+    def last_tiles(self, per_owner):
+        last = len(slot_kinds) - 1
+        tiles = []
+        for d in range(2):
+            f, half = self.piece(last, self.behind[d], d)
+            tiles.append(f * 2 + half)
+        return self.live(last, self.behind[0]), tiles, [lax.div(q, per_owner) == self.me_t for q in tiles]
+
+
 def routed_kernel(
-    n_fs, n_tp, tokens, gain, up_l, dn_l, up_w, dn_w, recv, x, hid, part, stage, up_f, dn_f, gain_v, acc,
+    n_fs, n_tp, tokens, gain, up_l, dn_l, up_w, dn_w, recv, hid, x, part, stage, up_f, dn_f, gain_v, acc,
     loc_sem, tok_s, tok_r, ring_s, ring_r, y_s, y_r, pre_s, pre_r, rs_s, rs_r,
 ):
-    nz, ny = grid_of(n_fs)
-    me_f, me_t = lax.axis_index("fs"), lax.axis_index("tp")
+    here = Places(n_fs, n_tp)
+    me_f, me_t, me_x, me_c, pos, at = here.me_f, here.me_t, here.me_x, here.me_c, here.pos, here.at
+    seat, behind, mirrored, piece, live = here.seat, here.behind, here.mirrored, here.piece, here.live
     T, Dk = tokens.shape
     R, F = up_l.shape
     D = n_fs * R
     W = R // 2
     nx = n_tp // 2
-    me_x, me_c = lax.div(me_t, 2), lax.rem(me_t, 2)
     sibling = me_t + 1 - 2 * me_c
     half_rows = T // 2
     per_owner = Dk // W
     S = len(slot_kinds)
     last = S - 1
 
-    mz, my = lax.div(me_f, ny), lax.rem(me_f, ny)
-    lane = mz + me_x * (nz - 1 - 2 * mz)
-    pos = lane + my * (n_fs - 1 - 2 * lane)
-
-    def at(p):
-        side = lax.div(p, nz)
-        along = p + side * (n_fs - 1 - 2 * p)
-        return (along + me_x * (nz - 1 - 2 * along)) * ny + side
-
     right, left, across = at(lax.rem(pos + 1, n_fs)), at(lax.rem(pos + n_fs - 1, n_fs)), at(n_fs - 1 - pos)
-    seat = (pos, n_fs - 1 - pos)
-    behind = tuple(lax.rem(p + n_fs - 1, n_fs) for p in seat)
     is_relay = (pos == relay_place) | (pos == n_fs - 1 - relay_place)
 
     def tp_peer(k):
@@ -392,24 +440,19 @@
     def tok_cols(t):
         return x.at[:, pl.ds(pl.multiple_of(t * Dk, Dk), Dk)]
 
+    quarter = W // 2
     gain_copy = pltpu.make_async_copy(gain, gain_v, loc_sem.at[0])
-    up_copies = [
-        pltpu.make_async_copy(up_l.at[pl.ds(h * W, W), :], up_f.at[pl.ds(h * W, W), :], loc_sem.at[1 + h]) for h in range(2)
-    ]
-    tok_copy = pltpu.make_async_copy(tokens, tok_cols(me_t), loc_sem.at[3])
-    dn_copy = pltpu.make_async_copy(dn_l, dn_f, loc_sem.at[4])
-    for c in [gain_copy] + up_copies + [dn_copy, tok_copy]:
-        c.start()
-
-    def mirrored(code, m):
-        src, half = lax.div(code, 2), lax.rem(code, 2)
-        return at(src + m * (n_fs - 1 - 2 * src)), half + m * (1 - 2 * half)
-
-    def piece(s, place, d):
-        return mirrored(look(slot_pieces[s], place, 4), d)
-
-    def live(s, place):
-        return None if slot_live[s] == 2**n_fs - 1 else look(slot_live[s], place, 1) == 1
+    firsts = [(h, c) for c in range(2) for h in range(2)]
+
+    def up_copy(h, c):
+        rows = pl.ds(h * W + c * quarter, quarter)
+        return pltpu.make_async_copy(up_l.at[rows, :], up_f.at[rows, :], loc_sem.at[1 + 2 * h + c])
+
+    tok_copy = pltpu.make_async_copy(tokens, tok_cols(me_t), loc_sem.at[5])
+    dn_copy = pltpu.make_async_copy(dn_l, dn_f, loc_sem.at[6])
+    gain_copy.start()
+    for h, c in firsts:
+        up_copy(h, c).start()
 
     def when(pred, body):
         if pred is None:
@@ -437,8 +480,8 @@
             device_id={"fs": right if d == 0 else left, "tp": me_t}, device_id_type=MESH,
         )
 
-    def send(s, c):
-        for d in range(2):
+    def send(s, c, sides=(0, 1)):
+        for d in sides:
             when(live(s, seat[d]), lambda: ring_copy(s, c, d, seat[d]).start())
 
     def arrive(s, c):
@@ -456,20 +499,33 @@
     relay_out = jnp.where(pos == relay_place, 0, 1)
 
     own_row = pl.multiple_of(me_f * R, R)
+    early_core = jnp.where(me_c == me_x, 0, 1)
+    leads = [look(second_leads, seat[d], 1) == early_core for d in range(2)]
     gain_copy.wait()
     spread = jnp.transpose(jnp.broadcast_to(gain_v[...], (128, R)))
-    for h in range(2):
-        up_copies[h].wait()
-        for c in range(F // 128):
-            cols = pl.ds(c * 128, 128)
-            up_w[pl.ds(own_row + h * W, W), cols] = (
-                spread[h * W : (h + 1) * W] * up_f[pl.ds(h * W, W), cols]
+
+    def convert(h, c):
+        up_copy(h, c).wait()
+        first = h * W + c * quarter
+        for j in range(F // 128):
+            cols = pl.ds(j * 128, 128)
+            up_w[pl.ds(own_row + first, quarter), cols] = (
+                spread[first : first + quarter] * up_f[pl.ds(first, quarter), cols]
             ).astype(jnp.bfloat16)
-    pl.semaphore_wait(barrier, n_tp + 2)
-    for t in range(2):
-        if t < slot_ahead[t]:
+
+    for h, c in firsts:
+        convert(h, c)
+        if (h, c) == (0, 0):
+            pl.semaphore_wait(barrier, n_tp + 2)
+        pl.when(leads[h])(lambda: send(0, c, (h,)))
+        if (h, c) == (1, 0):
+            tok_copy.start()
+            dn_copy.start()
+    for d in range(2):
+        @pl.when(leads[d])
+        def _():
             for e in range(2):
-                send(t, e)
+                send(1, e, (d,))
 
     def token_copy(k):
         return pltpu.make_async_remote_copy(
@@ -487,6 +543,13 @@
     def _(i):
         r = pl.ds(pl.multiple_of(i * block, block), block)
         dn_w[r, pl.ds(own_row, R)] = jnp.transpose(dn_f[:, r]).astype(jnp.bfloat16)
+
+    for d in range(2):
+        @pl.when(jnp.logical_not(leads[d]))
+        def _():
+            for t in range(2):
+                for e in range(2):
+                    send(t, e, (d,))
 
     def normalise():
         for k in range(1, n_tp):
@@ -552,21 +615,28 @@
             part[q, my_half, :] = both.astype(jnp.bfloat16)
             half_copy(q).start()
 
-    def do_part(q):
-        owner = lax.div(q, per_owner)
+    def do_pair(q, ok):
+        use = [jnp.where(ok[0] == 1, q[0], q[1]), jnp.where(ok[1] == 1, q[1], q[0])]
 
         @pl.loop(0, 2)
         def _(i):
             r = pl.ds(pl.multiple_of(lax.rem(i + 1 + me_c, 2) * half_rows, half_rows), half_rows)
-            part[q, r, :] = jnp.dot(hid[r, :], dn_w[:, tile(q)], preferred_element_type=jnp.float32).astype(jnp.bfloat16)
-
-            @pl.when((i == 0) & (lax.div(owner, nx) != me_x))
-            def _():
-                pair_copy(q).start()
-
-            @pl.when((i == 1) & (owner == sibling))
-            def _():
-                whole_copy(q).start()
+            both = jnp.concatenate([dn_w[:, tile(u)] for u in use], axis=1)
+            out = jnp.dot(hid[r, :], both, preferred_element_type=jnp.float32).astype(jnp.bfloat16)
+            for j in range(2):
+                owner = lax.div(q[j], per_owner)
+
+                @pl.when(ok[j] == 1)
+                def _():
+                    part[q[j], r, :] = out[:, j * W : (j + 1) * W]
+
+                    @pl.when((i == 0) & (lax.div(owner, nx) != me_x))
+                    def _():
+                        pair_copy(q[j]).start()
+
+                    @pl.when((i == 1) & (owner == sibling))
+                    def _():
+                        whole_copy(q[j]).start()
 
     def entry_of(e):
         kind = e[0]
@@ -588,77 +658,146 @@
             out = jnp.where(i == k, values[k], out)
         return out
 
-    def run_tiles(before, entries):
-        cur = [entry_of(e) for e in entries]
-        prev = [entry_of(before)] + cur[:-1]
-
-        @pl.loop(0, len(entries))
+    def pass_pair(q, ok):
+        for j in range(2):
+            @pl.when(ok[j] == 1)
+            def _():
+                pass_on(q[j])
+
+    def run_tiles(before, pairs):
+        cur = [[entry_of(e) for e in pair] for pair in pairs]
+        prev = [[entry_of(e) for e in before]] + cur[:-1]
+
+        @pl.loop(0, len(pairs))
         def _(i):
-            q = pick(i, [v[0] for v in cur])
-
-            @pl.when(pick(i, [v[1] for v in cur]) == 1)
+            def chosen(table, j, what):
+                return pick(i, [pair[j][what] for pair in table])
+
+            q, ok = [[chosen(cur, j, what) for j in range(2)] for what in range(2)]
+
+            @pl.when(ok[0] + ok[1] > 0)
             def _():
-                do_part(q)
-
-            p = pick(i, [v[0] for v in prev])
-
-            @pl.when(pick(i, [v[1] for v in prev]) == 1)
+                do_pair(q, ok)
+
+            pass_pair(*[[chosen(prev, j, what) for j in range(2)] for what in range(2)])
+
+    tail_on, tail_q, tail_mine = here.last_tiles(per_owner)
+    depth = F // last_chunks
+
+    def last_slot():
+        theirs = [tail_on & jnp.logical_not(m) for m in tail_mine]
+        for c in range(last_chunks):
+            k = pl.ds(c * depth, depth)
+            if c == 2:
+                settle()
+            for d in range(2):
+                @pl.when(theirs[d])
+                def _():
+                    q = tail_q[d]
+                    ring_copy(last, c, d, behind[d]).wait_recv()
+
+                    @pl.loop(0, 2)
+                    def _(i):
+                        r = pl.ds(pl.multiple_of(i * half_rows, half_rows), half_rows)
+                        out = jnp.dot(hid[r, k], dn_w[k, tile(q)], preferred_element_type=jnp.float32)
+                        if c > 0:
+                            out += acc[d, r, :]
+                        if c < last_chunks - 1:
+                            acc[d, r, :] = out
+                        else:
+                            part[q, r, :] = out.astype(jnp.bfloat16)
+
+                    if c == last_chunks - 1:
+                        whole_copy(q).start()
+
+        for d in range(2):
+            @pl.when(tail_on & tail_mine[d])
             def _():
-                pass_on(p)
-
-    def tail_tiles(c):
-        tiles = []
-        for d in range(2):
-            f, half = piece(last, behind[d], d)
-            tiles.append(f * 2 + half)
-        rows = half_rows
-        k = pl.ds(c * (F // last_chunks), F // last_chunks)
-
-        def body():
-            both = jnp.concatenate([dn_w[k, tile(q)] for q in tiles], axis=1)
-
-            @pl.loop(0, T // rows)
-            def _(i):
-                r = pl.ds(pl.multiple_of(i * rows, rows), rows)
-                out = jnp.dot(hid[r, k], both, preferred_element_type=jnp.float32)
-                if c > 0:
-                    out += acc[r, :]
-                if c < last_chunks - 1:
-                    acc[r, :] = out
-                else:
-                    for j, q in enumerate(tiles):
-                        part[q, r, :] = out[:, j * W : (j + 1) * W].astype(jnp.bfloat16)
-
-            if c == last_chunks - 1:
-                for q in tiles:
-                    @pl.when(lax.div(q, per_owner) == sibling)
-                    def _():
-                        whole_copy(q).start()
-
-        when(live(last, behind[0]), body)
+                for c in range(last_chunks):
+                    ring_copy(last, c, d, behind[d]).wait_recv()
+
+    def in_tail(q):
+        return tail_on & ((q == tail_q[0]) | (q == tail_q[1]))
+
+    def settle():
+        @pl.loop(0, per_owner)
+        def _(local):
+            q = me_t * per_owner + local
+
+            @pl.when(jnp.logical_not(in_tail(q)))
+            def _():
+                recv[me_x, :, cols_of(q)] = part[q]
+                whole_copy(q).wait_recv()
+
+            @pl.when(in_tail(q))
+            def _():
+                recv[me_x, :, cols_of(q)] = jnp.zeros((T, W), jnp.bfloat16)
+
+        for local in range(per_owner):
+            for k in range(1, nx):
+                src = lax.rem(me_x + k, nx)
+                for c in range(2):
+                    ref = recv.at[src, pl.ds(c * half_rows, half_rows), pl.ds(local * W, W)]
+                    pltpu.make_async_remote_copy(
+                        src_ref=ref, dst_ref=ref, send_sem=rs_s.at[0], recv_sem=rs_r.at[src, local, c], **device(sibling),
+                    ).wait_recv()
+
+        @pl.loop(0, D // W)
+        def _(q):
+            owner = lax.div(q, per_owner)
+
+            @pl.when((owner == sibling) & jnp.logical_not(in_tail(q)))
+            def _():
+                whole_copy(q).wait_send()
+
+            @pl.when(lax.div(owner, nx) != me_x)
+            def _():
+                pair_copy(q).wait_send()
+                half_copy(q).wait_send()
+
+        for j in range(len(relays)):
+            @pl.when(is_relay)
+            def _():
+                relay_copy(j, relay_out).wait_send()
+
+    def wait_sends(slots):
+        for s in slots:
+            for c in range(chunks(s)):
+                for d in range(2):
+                    when(live(s, seat[d]), lambda: ring_copy(s, c, d, seat[d]).wait_send())
 
     def send_after(t, e):
         if t == last:
             return (t - 1, 0)
         return (t - slot_ahead[t], e)
 
-    queue = [("own", h) for h in range(2)]
+    queue = [[("own", h) for h in range(2)]]
     hidden_from = 2 * max(s for s in range(S) if slot_kinds[s] == "U") + 1
     blocks = F // width
     per_step = (blocks + 1) // 2
-    prior = ("none",)
+    prior = [("none",)] * 2
     normal_at = max(0, hidden_from - 6)
 
     for s in range(S):
         for c in range(chunks(s)):
             k = index(s, c)
+            if s == last:
+                if c == 0:
+                    wait_sends(range(last - 2))
+                    last_slot()
+                continue
             arrive(s, c)
             for j, (t, _) in enumerate(relays):
                 if t + 1 == s and c == 0:
                     @pl.when(is_relay)
                     def _():
                         relay_copy(j, 1 - relay_out).wait_recv()
-                    queue.append(("relay", j))
+                    if j % 2 == 0:
+                        queue.append([("relay", j), ("none",)])
+                    elif queue and queue[-1][0] == ("relay", j - 1):
+                        queue[-1][1] = ("relay", j)
+                    else:
+                        queue.append([("relay", j), ("none",)])
             for t in range(s + 1, S):
                 for e in range(chunks(t)):
                     if send_after(t, e) == (s, c):
@@ -670,73 +809,47 @@
                         def _():
                             relay_copy(j, relay_out).start()
                 if slot_kinds[s] == "D":
-                    queue += [("ring", s, d) for d in range(2)]
+                    queue.append([("ring", s, d) for d in range(2)])
             if k == normal_at:
                 normalise()
             if k in (hidden_from, hidden_from + 1):
                 make_hidden((k - hidden_from) * per_step, min(per_step, blocks - (k - hidden_from) * per_step))
-            if k > hidden_from + 1 and (s, c) < (last - 1, 1) and queue:
-                take = queue[:tiles_per_step]
-                queue = queue[tiles_per_step:]
+            if k > hidden_from + 1 and queue:
+                count = len(queue) if (s, c) == (last - 1, 1) else pairs_per_step
+                take, queue = queue[:count], queue[count:]
                 run_tiles(prior, take)
                 prior = take[-1]
-            if (s, c) == (last - 1, 1):
-                if queue:
-                    run_tiles(prior, queue)
-                    prior = queue[-1]
-                    queue = []
-                q, ok = entry_of(prior)
-
-                @pl.when(ok == 1)
-                def _():
-                    pass_on(q)
-            if s == last:
-                tail_tiles(c)
-
-    @pl.loop(0, per_owner)
-    def _(local):
-        cols = pl.ds(pl.multiple_of(local * W, W), W)
-        recv[me_x, :, cols] = part[me_t * per_owner + local]
-
-    for s in range(S):
-        for c in range(chunks(s)):
-            for d in range(2):
-                when(live(s, seat[d]), lambda: ring_copy(s, c, d, seat[d]).wait_send())
-    for j in range(len(relays)):
-        @pl.when(is_relay)
+                if not queue:
+                    final = [entry_of(e) for e in prior]
+                    pass_pair([e[0] for e in final], [e[1] for e in final])
+                    prior = [("none",)] * 2
+
+    wait_sends(range(last - 2, S))
+    for d in range(2):
+        @pl.when(tail_on & (lax.div(tail_q[d], per_owner) == sibling))
         def _():
-            relay_copy(j, relay_out).wait_send()
-
-    @pl.loop(0, D // W)
-    def _(q):
-        owner = lax.div(q, per_owner)
-
-        @pl.when(owner == sibling)
+            whole_copy(tail_q[d]).wait_send()
+
+        @pl.when(tail_on & tail_mine[d])
         def _():
-            whole_copy(q).wait_send()
-
-        @pl.when(lax.div(owner, nx) != me_x)
-        def _():
-            pair_copy(q).wait_send()
-            half_copy(q).wait_send()
-
-    for local in range(per_owner):
-        q = me_t * per_owner + local
-        whole_copy(q).wait_recv()
-        for k in range(1, nx):
-            src = lax.rem(me_x + k, nx)
-            for c in range(2):
-                ref = recv.at[src, pl.ds(c * half_rows, half_rows), pl.ds(local * W, W)]
-                pltpu.make_async_remote_copy(
-                    src_ref=ref, dst_ref=ref, send_sem=rs_s.at[0], recv_sem=rs_r.at[src, local, c], **device(sibling),
-                ).wait_recv()
-
-
-def finish_kernel(up_v, dn_v, recv, up_o, dn_o, mlp_o, total, sem):
-    copies = [pltpu.make_async_copy(up_v, up_o, sem.at[0]), pltpu.make_async_copy(dn_v, dn_o, sem.at[1])]
+            whole_copy(tail_q[d]).wait_recv()
+
+
+def routed_finish(n_fs, n_tp, up_v, dn_v, recv, hid, up_o, dn_o, mlp_o, total, out, sem):
+    here = Places(n_fs, n_tp)
+    n, T, Dk = recv.shape
+    W = up_v.shape[0] // n_fs // 2
+    per_owner = Dk // W
+    copies = []
+    for k, (v, o) in enumerate(((up_v, up_o), (dn_v, dn_o))):
+        half = v.shape[0] // 2
+        copies += [
+            pltpu.make_async_copy(v.at[pl.ds(h * half, half), :], o.at[pl.ds(h * half, half), :], sem.at[2 * k + h])
+            for h in range(2)
+        ]
     for c in copies:
         c.start()
-    n, T, _ = recv.shape
+    tail_on, tail_q, tail_mine = here.last_tiles(per_owner)
     rows = 128
 
     @pl.loop(0, T // rows)
@@ -745,18 +858,91 @@
         acc = recv[0, r, :].astype(jnp.float32)
         for k in range(1, n):
             acc += recv[k, r, :].astype(jnp.float32)
-        total[r, :] = acc.astype(jnp.bfloat16)
-
-    last = pltpu.make_async_copy(total, mlp_o, sem.at[2])
-    last.start()
+        total[r, :] = acc
+
+    for d in range(2):
+        @pl.when(tail_on & tail_mine[d])
+        def _():
+            q = tail_q[d]
+            cols = pl.ds(pl.multiple_of(lax.rem(q, per_owner) * W, W), W)
+            own = dn_v.at[:, pl.ds(pl.multiple_of(q * W, W), W)]
+
+            @pl.loop(0, 2)
+            def _(i):
+                r = pl.ds(pl.multiple_of(i * (T // 2), T // 2), T // 2)
+                last = jnp.dot(hid[r, :], own[...], preferred_element_type=jnp.float32).astype(jnp.bfloat16)
+                total[r, cols] += last.astype(jnp.float32)
+
+    @pl.loop(0, T // rows)
+    def _(i):
+        r = pl.ds(pl.multiple_of(i * rows, rows), rows)
+        out[r, :] = total[r, :].astype(jnp.bfloat16)
+
+    written = pltpu.make_async_copy(out, mlp_o, sem.at[4])
+    written.start()
     for c in copies:
         c.wait()
-    last.wait()
+    written.wait()
 
 
 def solution(mesh):
     n_fs, n_tp = mesh.shape["fs"], mesh.shape["tp"]
     bf16 = jnp.bfloat16
+
+    def routed(tokens, norm_gain, up_master, down_master):
+        T, Dk = tokens.shape
+        R, F = up_master.shape
+        D, W = n_fs * R, R // 2
+        waves = 2 * len(slot_kinds) + last_chunks - 2
+        hbm_spec = pl.BlockSpec(memory_space=pltpu.HBM)
+        vmem_spec = pl.BlockSpec(memory_space=pltpu.VMEM)
+        dma = pltpu.SemaphoreType.DMA
+        held = pl.pallas_call(
+            functools.partial(routed_kernel, n_fs, n_tp),
+            out_shape=(
+                pltpu.VMEM((D, F), bf16),
+                pltpu.VMEM((F, D), bf16),
+                pltpu.VMEM((n_tp // 2 + 1, T, Dk), bf16),
+                pltpu.VMEM((T, F), bf16),
+            ),
+            in_specs=[hbm_spec] * 4,
+            out_specs=(vmem_spec,) * 4,
+            scratch_shapes=[
+                pltpu.VMEM((T, D), bf16),
+                pltpu.VMEM((D // W, T, W), bf16),
+                pltpu.VMEM((D // W, T // 2, W), bf16),
+                pltpu.VMEM((R, F), jnp.float32),
+                pltpu.VMEM((R, F), jnp.float32),
+                pltpu.VMEM((1, R), jnp.float32),
+                pltpu.VMEM((2, T, W), jnp.float32),
+                dma((7,)),
+                dma((n_tp,)),
+                dma((n_tp,)),
+                dma((2, waves)),
+                dma((2, waves)),
+                dma((len(relays),)),
+                dma((len(relays),)),
+                dma((D // W,)),
+                dma((D // W,)),
+                dma((D // W,)),
+                dma((n_tp // 2 + 1, Dk // W, 2)),
+            ],
+            compiler_params=pltpu.CompilerParams(
+                collective_id=0, has_side_effects=True, vmem_limit_bytes=40 * 2**20
+            ),
+        )(tokens, norm_gain[None, :], up_master, down_master)
+        return pl.pallas_call(
+            functools.partial(routed_finish, n_fs, n_tp),
+            out_shape=(
+                jax.ShapeDtypeStruct((D, F), bf16),
+                jax.ShapeDtypeStruct((F, D), bf16),
+                jax.ShapeDtypeStruct((T, Dk), bf16),
+            ),
+            in_specs=[vmem_spec] * 4,
+            out_specs=(pl.BlockSpec(memory_space=pl.ANY),) * 3,
+            scratch_shapes=[pltpu.VMEM((T, Dk), jnp.float32), pltpu.VMEM((T, Dk), bf16), dma((5,))],
+            compiler_params=pltpu.CompilerParams(vmem_limit_bytes=12 * 2**20),
+        )(*held)
 
     def on_device(tokens, norm_gain, up_master, down_master):
         T, Dk = tokens.shape
@@ -766,13 +952,10 @@
         S = len(send_list(n_fs))
         any_spec = pl.BlockSpec(memory_space=pl.ANY)
         vmem_spec = pl.BlockSpec(memory_space=pltpu.VMEM)
-        routed = (n_fs, grid_of(n_fs)[1], n_tp * grid_of(n_fs)[1], 2 * W) == (ring_places, 2, n_fs, R)
-        waves = 2 * len(slot_kinds) + last_chunks - 2 if routed else S
-        own_sems = 5 if routed else 4
-        extra = [pltpu.VMEM((T, 2 * W), jnp.float32)] if routed else []
-        relay_sems = [pltpu.SemaphoreType.DMA((len(relays),))] * 2 if routed else []
+        if (n_fs, grid_of(n_fs)[1], n_tp * grid_of(n_fs)[1], 2 * W) == (ring_places, 2, n_fs, R):
+            return routed(tokens, norm_gain, up_master, down_master)
         up_v, dn_v, recv = pl.pallas_call(
-            functools.partial(routed_kernel if routed else gather_kernel, n_fs, n_tp),
+            functools.partial(gather_kernel, n_fs, n_tp),
             out_shape=(pltpu.VMEM((D, F), bf16), pltpu.VMEM((F, D), bf16), pltpu.VMEM((n_tp // 2 + 1, T, Dk), bf16)),
             in_specs=[pl.BlockSpec(memory_space=pltpu.HBM)] * 4,
             out_specs=(vmem_spec,) * 3,
@@ -784,13 +967,11 @@
                 pltpu.VMEM((R, F), jnp.float32),
                 pltpu.VMEM((R, F), jnp.float32),
                 pltpu.VMEM((1, R), jnp.float32),
-                *extra,
-                pltpu.SemaphoreType.DMA((own_sems,)),
+                pltpu.SemaphoreType.DMA((4,)),
                 pltpu.SemaphoreType.DMA((n_tp,)),
                 pltpu.SemaphoreType.DMA((n_tp,)),
-                pltpu.SemaphoreType.DMA((2, waves)),
-                pltpu.SemaphoreType.DMA((2, waves)),
-                *relay_sems,
+                pltpu.SemaphoreType.DMA((2, S)),
+                pltpu.SemaphoreType.DMA((2, S)),
                 pltpu.SemaphoreType.DMA((D // W,)),
                 pltpu.SemaphoreType.DMA((D // W,)),
                 pltpu.SemaphoreType.DMA((D // W,)),

time: 174 us -> 173 us (level)
  no operation moved by 1% of the time
where the time goes in v2:
time: 173 us
  Pallas kernels  172 us (99%)
    pallas_call x1, Pallas kernels, routed(): pl.pallas_call(functools.partial(routed_kernel, n_fs, n_tp), out_shape=(p...  166 us
    pallas_call x1, Pallas kernels, routed(): pl.pallas_call(functools.partial(routed_finish, n_fs, n_tp), out_shape=(j...  6.18 us

profile of v2, /device:TPU:1, one launch (start us, length us, event | category | flops | bytes accessed | tf_op | source)
XLA Modules:
  0.0 172.6 jit_solution(13282690021989879577)
XLA Ops:
  0.6 165.8 %shard_map.67 = (bf16[2048,2048]{1,0:T(8,128)(2,1)S(1)}, bf16[2048,2048]{1,0:T(8,128)(2,1)S(1)}, bf16[3,1024,512]{2,1,0:T(8,128)(2,1)S(1)}, bf16[1024,2048]{1,0:T(8,128)(2,1)S(1)}) custom-call(bf16[1024,512]{1,0:T(8,128)(2,1)} %tokens.1, f32[1,256]{1,0:T(1,128)} %bitcast.1, f32[256,2048]{1,0:T(8,128)} %up_l.1, f32[256,2048]{1,0:T(8,128)} %dn_l.1), custom_call_target="tpu_custom_call" | custom-call | tf_op jit(solution)/shard_map/pallas_call | solution.py:900
  166.5 6.2 %shard_map.68 = (bf16[2048,2048]{1,0:T(8,128)(2,1)}, bf16[2048,2048]{1,0:T(8,128)(2,1)}, bf16[1024,512]{1,0:T(8,128)(2,1)}) custom-call(bf16[2048,2048]{1,0:T(8,128)(2,1)S(1)} %get-tuple-element.7.up_v, bf16[2048,2048]{1,0:T(8,128)(2,1)S(1)} %get-tuple-element.8.dn_v, bf16[3,1024,512]{2,1,0:T(8,128)(2,1)S(1)} %get-tuple-element.9.recv, ...), custom_call_target="tpu_custom_call" | custom-call | tf_op jit(solution)/shard_map/pallas_call | solution.py:934

commit v3 on v2

--- a/solution.py
+++ b/solution.py
@@ -349,20 +349,20 @@
 slot_kinds = "UUDUUDUUUDDDDD"
 slot_pieces = (
     0xECA86420, 0xFDB97531,
-    0xECA96420, 0xCA86420E,
-    0xDB97531F, 0xCAB87501,
+    0xECA86420, 0xCA86420E,
+    0xDB97531F, 0xFAB97531,
     0xA86420EC, 0xB97531FD,
-    0x86420ECA, 0xAB87423E,
-    0xB896501C, 0x897423EA,
-    0x926501F0, 0xFD023EC0,
+    0x86420ECA, 0xAB97420E,
+    0xB986531F, 0x987420EA,
+    0x826531F0, 0xCD020EC0,
 )
 slot_live = (0xFF, 0xFF, 0xFF, 0xFF, 0xFF, 0xFF, 0xFF, 0xFF, 0xFF, 0xFF, 0xFF, 0xFF, 0xFE, 0xDE)
-slot_ahead = (1, 2, 2, 2, 2, 2, 2, 2, 2, 2, 1, 1, 1, 2)
-relays = ((1, 13), (4, 15), (7, 11))
+slot_tight = (0x00, 0x00, 0x00, 0x00, 0x00, 0x00, 0x00, 0x00, 0x00, 0x00, 0xC0, 0xC0, 0x80, 0x00)
+relays = ((1, 12), (2, 13), (7, 11))
 relay_place = 6
 ring_places = 8
 last_chunks = 4
-second_leads = 0x84
+second_leads = 0x0C
 pairs_per_step = 2
 
 
@@ -404,7 +404,7 @@
         for d in range(2):
             f, half = self.piece(last, self.behind[d], d)
             tiles.append(f * 2 + half)
-        return self.live(last, self.behind[0]), tiles, [lax.div(q, per_owner) == self.me_t for q in tiles]
+        return self.live(last, self.behind[0]), tiles, lax.div(tiles[0], per_owner) == self.me_t
 
 
 def routed_kernel(
@@ -480,9 +480,13 @@
             device_id={"fs": right if d == 0 else left, "tp": me_t}, device_id_type=MESH,
         )
 
-    def send(s, c, sides=(0, 1)):
+    def send(s, c, sides=(0, 1), tight=None):
         for d in sides:
-            when(live(s, seat[d]), lambda: ring_copy(s, c, d, seat[d]).start())
+            pred = live(s, seat[d])
+            if tight is not None:
+                here_tight = (look(slot_tight[s], seat[d], 1) == 1) == tight
+                pred = here_tight if pred is None else pred & here_tight
+            when(pred, lambda: ring_copy(s, c, d, seat[d]).start())
 
     def arrive(s, c):
         for d in range(2):
@@ -539,9 +543,9 @@
     dn_copy.wait()
     block = min(F, 256)
 
-    @pl.loop(0, F // block)
+    @pl.loop(0, 2 * (F // block))
     def _(i):
-        r = pl.ds(pl.multiple_of(i * block, block), block)
+        r = pl.ds(pl.multiple_of(lax.rem(i, F // block) * block, block), block)
         dn_w[r, pl.ds(own_row, R)] = jnp.transpose(dn_f[:, r]).astype(jnp.bfloat16)
 
     for d in range(2):
@@ -684,36 +688,40 @@
     tail_on, tail_q, tail_mine = here.last_tiles(per_owner)
     depth = F // last_chunks
 
+    def across_copy(q, i):
+        r = pl.ds(i * half_rows, half_rows)
+        return pltpu.make_async_remote_copy(
+            src_ref=part.at[q, r], dst_ref=recv.at[nx, r, cols_of(q)],
+            send_sem=(rs_s, pre_s)[i].at[q], recv_sem=rs_r.at[nx, lax.rem(q, per_owner), i], **device(sibling),
+        )
+
     def last_slot():
-        theirs = [tail_on & jnp.logical_not(m) for m in tail_mine]
         for c in range(last_chunks):
             k = pl.ds(c * depth, depth)
-            if c == 2:
-                settle()
-            for d in range(2):
-                @pl.when(theirs[d])
-                def _():
-                    q = tail_q[d]
+            @pl.when(tail_on & jnp.logical_not(tail_mine))
+            def _():
+                for d in range(2):
                     ring_copy(last, c, d, behind[d]).wait_recv()
-
-                    @pl.loop(0, 2)
-                    def _(i):
-                        r = pl.ds(pl.multiple_of(i * half_rows, half_rows), half_rows)
-                        out = jnp.dot(hid[r, k], dn_w[k, tile(q)], preferred_element_type=jnp.float32)
-                        if c > 0:
-                            out += acc[d, r, :]
-                        if c < last_chunks - 1:
-                            acc[d, r, :] = out
-                        else:
-                            part[q, r, :] = out.astype(jnp.bfloat16)
-
-                    if c == last_chunks - 1:
-                        whole_copy(q).start()
-
-        for d in range(2):
-            @pl.when(tail_on & tail_mine[d])
-            def _():
-                for c in range(last_chunks):
+                for i in range(2):
+                    r = pl.ds(i * half_rows, half_rows)
+                    both = jnp.concatenate([dn_w[k, tile(q)] for q in tail_q], axis=1)
+                    out = jnp.dot(hid[r, k], both, preferred_element_type=jnp.float32)
+                    if c > 0:
+                        out += acc[r, :]
+                    if c < last_chunks - 1:
+                        acc[r, :] = out
+                    else:
+                        for j, q in enumerate(tail_q):
+                            part[q, r, :] = out[:, j * W : (j + 1) * W].astype(jnp.bfloat16)
+                        for q in tail_q:
+                            across_copy(q, i).start()
+
+        settle()
+
+        @pl.when(tail_on & tail_mine)
+        def _():
+            for c in range(last_chunks):
+                for d in range(2):
                     ring_copy(last, c, d, behind[d]).wait_recv()
 
     def in_tail(q):
@@ -766,10 +774,14 @@
                 for d in range(2):
                     when(live(s, seat[d]), lambda: ring_copy(s, c, d, seat[d]).wait_send())
 
-    def send_after(t, e):
-        if t == last:
-            return (t - 1, 0)
-        return (t - slot_ahead[t], e)
+    def sends_after(s, c):
+        if s + 1 < last and slot_tight[s + 1]:
+            send(s + 1, c, tight=True)
+        if s + 2 < last:
+            send(s + 2, c, tight=False if slot_tight[s + 2] else None)
+        if (s + 2, c) == (last, 1):
+            for e in range(last_chunks):
+                send(last, e)
 
     queue = [[("own", h) for h in range(2)]]
     hidden_from = 2 * max(s for s in range(S) if slot_kinds[s] == "U") + 1
@@ -798,10 +810,7 @@
                         queue[-1][1] = ("relay", j)
                     else:
                         queue.append([("relay", j), ("none",)])
-            for t in range(s + 1, S):
-                for e in range(chunks(t)):
-                    if send_after(t, e) == (s, c):
-                        send(t, e)
+            sends_after(s, c)
             if c == 1 and s < last:
                 for j, (t, _) in enumerate(relays):
                     if t == s + 1:
@@ -825,14 +834,18 @@
                     prior = [("none",)] * 2
 
     wait_sends(range(last - 2, S))
-    for d in range(2):
-        @pl.when(tail_on & (lax.div(tail_q[d], per_owner) == sibling))
-        def _():
-            whole_copy(tail_q[d]).wait_send()
-
-        @pl.when(tail_on & tail_mine[d])
-        def _():
-            whole_copy(tail_q[d]).wait_recv()
+
+    @pl.when(tail_on & jnp.logical_not(tail_mine))
+    def _():
+        for q in tail_q:
+            for i in range(2):
+                across_copy(q, i).wait_send()
+
+    @pl.when(tail_on & tail_mine)
+    def _():
+        for q in tail_q:
+            for i in range(2):
+                across_copy(q, i).wait_recv()
 
 
 def routed_finish(n_fs, n_tp, up_v, dn_v, recv, hid, up_o, dn_o, mlp_o, total, out, sem):
@@ -860,18 +873,16 @@
             acc += recv[k, r, :].astype(jnp.float32)
         total[r, :] = acc
 
-    for d in range(2):
-        @pl.when(tail_on & tail_mine[d])
-        def _():
-            q = tail_q[d]
-            cols = pl.ds(pl.multiple_of(lax.rem(q, per_owner) * W, W), W)
-            own = dn_v.at[:, pl.ds(pl.multiple_of(q * W, W), W)]
-
-            @pl.loop(0, 2)
-            def _(i):
-                r = pl.ds(pl.multiple_of(i * (T // 2), T // 2), T // 2)
-                last = jnp.dot(hid[r, :], own[...], preferred_element_type=jnp.float32).astype(jnp.bfloat16)
-                total[r, cols] += last.astype(jnp.float32)
+    @pl.when(tail_on & tail_mine)
+    def _():
+        @pl.loop(0, 2)
+        def _(i):
+            r = pl.ds(pl.multiple_of(i * (T // 2), T // 2), T // 2)
+            both = jnp.concatenate([dn_v[:, pl.ds(pl.multiple_of(q * W, W), W)] for q in tail_q], axis=1)
+            late = jnp.dot(hid[r, :], both, preferred_element_type=jnp.float32).astype(jnp.bfloat16)
+            for j, q in enumerate(tail_q):
+                cols = pl.ds(pl.multiple_of(lax.rem(q, per_owner) * W, W), W)
+                total[r, cols] += late[:, j * W : (j + 1) * W].astype(jnp.float32)
 
     @pl.loop(0, T // rows)
     def _(i):
@@ -914,7 +925,7 @@
                 pltpu.VMEM((R, F), jnp.float32),
                 pltpu.VMEM((R, F), jnp.float32),
                 pltpu.VMEM((1, R), jnp.float32),
-                pltpu.VMEM((2, T, W), jnp.float32),
+                pltpu.VMEM((T, 2 * W), jnp.float32),
                 dma((7,)),
                 dma((n_tp,)),
                 dma((n_tp,)),

time: 173 us -> 172 us (level)
  no operation moved by 1% of the time
where the time goes in v3:
time: 172 us
  Pallas kernels  171 us (99%)
    pallas_call x1, Pallas kernels, routed(): pl.pallas_call(functools.partial(routed_kernel, n_fs, n_tp), out_shape=(p...  165 us
    pallas_call x1, Pallas kernels, routed(): pl.pallas_call(functools.partial(routed_finish, n_fs, n_tp), out_shape=(j...  6.18 us

profile of v3, /device:TPU:1, one launch (start us, length us, event | category | flops | bytes accessed | tf_op | source)
XLA Modules:
  0.0 171.7 jit_solution(4366012898693093494)
XLA Ops:
  0.6 164.8 %shard_map.67 = (bf16[2048,2048]{1,0:T(8,128)(2,1)S(1)}, bf16[2048,2048]{1,0:T(8,128)(2,1)S(1)}, bf16[3,1024,512]{2,1,0:T(8,128)(2,1)S(1)}, bf16[1024,2048]{1,0:T(8,128)(2,1)S(1)}) custom-call(bf16[1024,512]{1,0:T(8,128)(2,1)} %tokens.1, f32[1,256]{1,0:T(1,128)} %bitcast.1, f32[256,2048]{1,0:T(8,128)} %up_l.1, f32[256,2048]{1,0:T(8,128)} %dn_l.1), custom_call_target="tpu_custom_call" | custom-call | tf_op jit(solution)/shard_map/pallas_call | solution.py:911
  165.5 6.2 %shard_map.68 = (bf16[2048,2048]{1,0:T(8,128)(2,1)}, bf16[2048,2048]{1,0:T(8,128)(2,1)}, bf16[1024,512]{1,0:T(8,128)(2,1)}) custom-call(bf16[2048,2048]{1,0:T(8,128)(2,1)S(1)} %get-tuple-element.7.up_v, bf16[2048,2048]{1,0:T(8,128)(2,1)S(1)} %get-tuple-element.8.dn_v, bf16[3,1024,512]{2,1,0:T(8,128)(2,1)S(1)} %get-tuple-element.9.recv, ...), custom_call_target="tpu_custom_call" | custom-call | tf_op jit(solution)/shard_map/pallas_call | solution.py:945

commit v4 on v3

--- a/solution.py
+++ b/solution.py
@@ -411,6 +411,20 @@
     n_fs, n_tp, tokens, gain, up_l, dn_l, up_w, dn_w, recv, hid, x, part, stage, up_f, dn_f, gain_v, acc,
     loc_sem, tok_s, tok_r, ring_s, ring_r, y_s, y_r, pre_s, pre_r, rs_s, rs_r,
 ):
+    R, F = up_l.shape
+    W = R // 2
+    quarter = W // 2
+    gain_copy = pltpu.make_async_copy(gain, gain_v, loc_sem.at[0])
+    firsts = [(h, c) for c in range(2) for h in range(2)]
+
+    def up_copy(h, c):
+        rows = pl.ds(h * W + c * quarter, quarter)
+        return pltpu.make_async_copy(up_l.at[rows, :], up_f.at[rows, :], loc_sem.at[1 + 2 * h + c])
+
+    gain_copy.start()
+    for h, c in firsts:
+        up_copy(h, c).start()
+
     here = Places(n_fs, n_tp)
     me_f, me_t, me_x, me_c, pos, at = here.me_f, here.me_t, here.me_x, here.me_c, here.pos, here.at
     seat, behind, mirrored, piece, live = here.seat, here.behind, here.mirrored, here.piece, here.live
@@ -440,19 +454,8 @@
     def tok_cols(t):
         return x.at[:, pl.ds(pl.multiple_of(t * Dk, Dk), Dk)]
 
-    quarter = W // 2
-    gain_copy = pltpu.make_async_copy(gain, gain_v, loc_sem.at[0])
-    firsts = [(h, c) for c in range(2) for h in range(2)]
-
-    def up_copy(h, c):
-        rows = pl.ds(h * W + c * quarter, quarter)
-        return pltpu.make_async_copy(up_l.at[rows, :], up_f.at[rows, :], loc_sem.at[1 + 2 * h + c])
-
     tok_copy = pltpu.make_async_copy(tokens, tok_cols(me_t), loc_sem.at[5])
     dn_copy = pltpu.make_async_copy(dn_l, dn_f, loc_sem.at[6])
-    gain_copy.start()
-    for h, c in firsts:
-        up_copy(h, c).start()
 
     def when(pred, body):
         if pred is None:
@@ -849,7 +852,6 @@
 
 
 def routed_finish(n_fs, n_tp, up_v, dn_v, recv, hid, up_o, dn_o, mlp_o, total, out, sem):
-    here = Places(n_fs, n_tp)
     n, T, Dk = recv.shape
     W = up_v.shape[0] // n_fs // 2
     per_owner = Dk // W
@@ -862,6 +864,7 @@
         ]
     for c in copies:
         c.start()
+    here = Places(n_fs, n_tp)
     tail_on, tail_q, tail_mine = here.last_tiles(per_owner)
     rows = 128
 

time: 172 us -> 172 us (level)
  no operation moved by 1% of the time
where the time goes in v4:
time: 172 us
  Pallas kernels  171 us (99%)
    pallas_call x1, Pallas kernels, routed(): pl.pallas_call(functools.partial(routed_kernel, n_fs, n_tp), out_shape=(p...  165 us
    pallas_call x1, Pallas kernels, routed(): pl.pallas_call(functools.partial(routed_finish, n_fs, n_tp), out_shape=(j...  6.18 us

profile of v4, /device:TPU:1, one launch (start us, length us, event | category | flops | bytes accessed | tf_op | source)
XLA Modules:
  0.0 171.7 jit_solution(6632040604974371267)
XLA Ops:
  0.6 164.8 %shard_map.67 = (bf16[2048,2048]{1,0:T(8,128)(2,1)S(1)}, bf16[2048,2048]{1,0:T(8,128)(2,1)S(1)}, bf16[3,1024,512]{2,1,0:T(8,128)(2,1)S(1)}, bf16[1024,2048]{1,0:T(8,128)(2,1)S(1)}) custom-call(bf16[1024,512]{1,0:T(8,128)(2,1)} %tokens.1, f32[1,256]{1,0:T(1,128)} %bitcast.1, f32[256,2048]{1,0:T(8,128)} %up_l.1, f32[256,2048]{1,0:T(8,128)} %dn_l.1), custom_call_target="tpu_custom_call" | custom-call | tf_op jit(solution)/shard_map/pallas_call | solution.py:914
  165.5 6.2 %shard_map.68 = (bf16[2048,2048]{1,0:T(8,128)(2,1)}, bf16[2048,2048]{1,0:T(8,128)(2,1)}, bf16[1024,512]{1,0:T(8,128)(2,1)}) custom-call(bf16[2048,2048]{1,0:T(8,128)(2,1)S(1)} %get-tuple-element.7.up_v, bf16[2048,2048]{1,0:T(8,128)(2,1)S(1)} %get-tuple-element.8.dn_v, bf16[3,1024,512]{2,1,0:T(8,128)(2,1)S(1)} %get-tuple-element.9.recv, ...), custom_call_target="tpu_custom_call" | custom-call | tf_op jit(solution)/shard_map/pallas_call | solution.py:948

commit v5 on v4

--- a/solution.py
+++ b/solution.py
@@ -720,6 +720,7 @@
                             across_copy(q, i).start()
 
         settle()
+        wait_sends(range(last - 2, last))
 
         @pl.when(tail_on & tail_mine)
         def _():
@@ -836,7 +837,7 @@
                     pass_pair([e[0] for e in final], [e[1] for e in final])
                     prior = [("none",)] * 2
 
-    wait_sends(range(last - 2, S))
+    wait_sends((last,))
 
     @pl.when(tail_on & jnp.logical_not(tail_mine))
     def _():

time: 172 us -> 172 us (level)
  no operation moved by 1% of the time
where the time goes in v5:
time: 172 us
  Pallas kernels  171 us (99%)
    pallas_call x1, Pallas kernels, routed(): pl.pallas_call(functools.partial(routed_kernel, n_fs, n_tp), out_shape=(p...  165 us
    pallas_call x1, Pallas kernels, routed(): pl.pallas_call(functools.partial(routed_finish, n_fs, n_tp), out_shape=(j...  6.18 us

profile of v5, /device:TPU:1, one launch (start us, length us, event | category | flops | bytes accessed | tf_op | source)
XLA Modules:
  0.0 171.6 jit_solution(10799351904206741938)
XLA Ops:
  0.6 164.8 %shard_map.67 = (bf16[2048,2048]{1,0:T(8,128)(2,1)S(1)}, bf16[2048,2048]{1,0:T(8,128)(2,1)S(1)}, bf16[3,1024,512]{2,1,0:T(8,128)(2,1)S(1)}, bf16[1024,2048]{1,0:T(8,128)(2,1)S(1)}) custom-call(bf16[1024,512]{1,0:T(8,128)(2,1)} %tokens.1, f32[1,256]{1,0:T(1,128)} %bitcast.1, f32[256,2048]{1,0:T(8,128)} %up_l.1, f32[256,2048]{1,0:T(8,128)} %dn_l.1), custom_call_target="tpu_custom_call" | custom-call | tf_op jit(solution)/shard_map/pallas_call | solution.py:915
  165.5 6.2 %shard_map.68 = (bf16[2048,2048]{1,0:T(8,128)(2,1)}, bf16[2048,2048]{1,0:T(8,128)(2,1)}, bf16[1024,512]{1,0:T(8,128)(2,1)}) custom-call(bf16[2048,2048]{1,0:T(8,128)(2,1)S(1)} %get-tuple-element.7.up_v, bf16[2048,2048]{1,0:T(8,128)(2,1)S(1)} %get-tuple-element.8.dn_v, bf16[3,1024,512]{2,1,0:T(8,128)(2,1)S(1)} %get-tuple-element.9.recv, ...), custom_call_target="tpu_custom_call" | custom-call | tf_op jit(solution)/shard_map/pallas_call | solution.py:949
